TPU v7x, 32 devices: a whole 2x2x4 slice. The times are simulated.
32 devices in a mesh: kv: 8 (over z, y), tp: 4 (over x, core).
Axes of the slice: x: 2, y: 2, z: 4, core: 2. Of those that a mesh axis runs over, the one named last changes fastest.
Arguments:
- residual: bfloat16 [256, 2048], P('kv', 'tp'), may hold values from -12 to 12
- first_gain: bfloat16 [2048], P('tp'), may hold values from 0.099609375 to 1.8984375
- first_gate: bfloat16 [2048, 5632], P('tp', 'kv'), may hold values from -0.125 to 0.125
- first_lift: bfloat16 [2048, 5632], P('tp', 'kv'), may hold values from -0.125 to 0.125
- first_down: bfloat16 [5632, 2048], P('kv', 'tp'), may hold values from -0.078125 to 0.078125
- mixer_gain: bfloat16 [2048], replicated, may hold values from 0.099609375 to 1.8984375
- proj_gate: bfloat16 [2048, 2048], P(None, 'tp'), may hold values from -0.125 to 0.125
- proj_input: bfloat16 [2048, 2048], P(None, 'tp'), may hold values from -0.125 to 0.125
- proj_write: bfloat16 [2048, 1024], P(None, 'tp'), may hold values from -0.125 to 0.125
- proj_read: bfloat16 [2048, 1024], P(None, 'tp'), may hold values from -0.125 to 0.125
- proj_step: bfloat16 [2048, 32], P(None, 'tp'), may hold values from -0.125 to 0.125
- step_bias: float32 [32], P('tp'), may hold values from -5 to -2
- rate_log: float32 [32], P('tp'), may hold values from -0.7 to 2.1
- skip_gain: float32 [32], P('tp'), may hold values from 0.5 to 2
- taps_input: bfloat16 [4, 2048], P(None, 'tp'), may hold values from -3 to 3
- taps_write: bfloat16 [4, 1024], P(None, 'tp'), may hold values from -3 to 3
- taps_read: bfloat16 [4, 1024], P(None, 'tp'), may hold values from -3 to 3
- buffer_input: bfloat16 [256, 3, 2048], P('kv', None, 'tp'), may hold values from -6 to 6
- buffer_write: bfloat16 [256, 3, 1024], P('kv', None, 'tp'), may hold values from -6 to 6
- buffer_read: bfloat16 [256, 3, 1024], P('kv', None, 'tp'), may hold values from -6 to 6
- scan_state: float32 [256, 32, 64, 128], P('kv', 'tp'), may hold values from -1.5 to 1.5
- group_gain: bfloat16 [2048], P('tp'), may hold values from 0.099609375 to 1.8984375
- proj_output: bfloat16 [2048, 2048], P('tp'), may hold values from -0.125 to 0.125
- second_gain: bfloat16 [2048], P('tp'), may hold values from 0.099609375 to 1.8984375
- second_gate: bfloat16 [2048, 5632], P('tp', 'kv'), may hold values from -0.125 to 0.125
- second_lift: bfloat16 [2048, 5632], P('tp', 'kv'), may hold values from -0.125 to 0.125
- second_down: bfloat16 [5632, 2048], P('kv', 'tp'), may hold values from -0.078125 to 0.078125
Outputs:
- residual_out: bfloat16 [256, 2048], P('kv', 'tp')
- state_out: float32 [256, 32, 64, 128], P('kv', 'tp')
All inputs are finite; a program needn't handle non-finite values.
Results may differ from a plain program's by a relative error of at most 0.023.
Values may be sent and summed in bfloat16 or wider, within the bound.
A program may use at most 64 MiB of HBM per device.

v0:
```python
import jax
import jax.numpy as jnp
from jax import lax
from jax.sharding import PartitionSpec as P

D = 2048
HEAD_DIM = 64
STATE = 128
norm_eps = 1e-06


def inverse_rms(values):
    return lax.rsqrt(jnp.mean(values * values, axis=-1, keepdims=True) + norm_eps)


def half_step(residual, gain, gate_weight, lift_weight, down_weight):
    widened = residual.astype(jnp.float32)
    row_total = lax.psum(jnp.sum(widened * widened, axis=1), "tp")
    factor = lax.rsqrt(row_total / D + norm_eps)
    normed = (widened * factor[:, None] * gain.astype(jnp.float32)[None, :]).astype(jnp.bfloat16)
    hidden_cols = gate_weight.shape[1]
    row_piece = lax.all_gather(normed, "kv", axis=0, tiled=True)
    gate_part = jnp.dot(row_piece, gate_weight, preferred_element_type=jnp.float32).astype(
        jnp.bfloat16
    )
    lift_part = jnp.dot(row_piece, lift_weight, preferred_element_type=jnp.float32).astype(
        jnp.bfloat16
    )
    joined = lax.optimization_barrier(jnp.concatenate([gate_part, lift_part], axis=1))
    partial_value = joined.astype(jnp.float32)
    share = lax.psum_scatter(
        partial_value.astype(jnp.bfloat16), "tp", scatter_dimension=0, tiled=True
    ).astype(jnp.float32)
    active = (jax.nn.silu(share[:, :hidden_cols]) * share[:, hidden_cols:]).astype(jnp.bfloat16)
    hidden = lax.all_gather(active, "tp", axis=0, tiled=True)
    branch = lax.psum_scatter(
        jnp.dot(hidden, down_weight, preferred_element_type=jnp.float32).astype(jnp.bfloat16),
        "kv",
        scatter_dimension=0,
        tiled=True,
    ).astype(jnp.float32)
    return (widened + 0.5 * branch).astype(jnp.bfloat16)


def short_conv(tap_weights, buffer, newest):
    taps_f = tap_weights.astype(jnp.float32)
    summed = jnp.sum(buffer.astype(jnp.float32) * taps_f[None, :-1, :], axis=1)
    summed = summed + newest.astype(jnp.float32) * taps_f[-1][None, :]
    return jax.nn.silu(summed)


def state_mixer(
    residual,
    mixer_gain,
    proj_gate,
    proj_input,
    proj_write,
    proj_read,
    proj_step,
    step_bias,
    rate_log,
    skip_gain,
    taps_input,
    taps_write,
    taps_read,
    buffer_input,
    buffer_write,
    buffer_read,
    scan_state,
    group_gain,
    proj_output,
):
    seq_rows = residual.shape[0]
    full_rows = lax.all_gather(residual, "tp", axis=1, tiled=True)
    widened = full_rows.astype(jnp.float32)
    normed = (widened * inverse_rms(widened) * mixer_gain.astype(jnp.float32)[None, :]).astype(
        jnp.bfloat16
    )

    def state_project(weight):
        return jnp.dot(normed, weight, preferred_element_type=jnp.float32).astype(jnp.bfloat16)

    gate_z = state_project(proj_gate)
    input_new = state_project(proj_input)
    write_new = state_project(proj_write)
    read_new = state_project(proj_read)
    step_raw = state_project(proj_step)
    input_conv = short_conv(taps_input, buffer_input, input_new)
    write_conv = short_conv(taps_write, buffer_write, write_new)
    read_conv = short_conv(taps_read, buffer_read, read_new)
    head_count = proj_step.shape[1]
    group_count = proj_write.shape[1] // STATE
    per_group = head_count // group_count
    step = jax.nn.softplus(step_raw.astype(jnp.float32) + step_bias[None, :])
    retain = jnp.exp(-step * jnp.exp(rate_log)[None, :])
    input_heads = input_conv.reshape(seq_rows, group_count, per_group, HEAD_DIM)
    write_groups = write_conv.reshape(seq_rows, group_count, STATE)
    read_groups = read_conv.reshape(seq_rows, group_count, STATE)
    old_state = scan_state.reshape(seq_rows, group_count, per_group, HEAD_DIM, STATE)
    retain_g = retain.reshape(seq_rows, group_count, per_group)
    step_g = step.reshape(seq_rows, group_count, per_group)
    updated = (
        retain_g[..., None, None] * old_state
        + (step_g[..., None] * input_heads)[..., None] * write_groups[:, :, None, None, :]
    )
    head_out = jnp.einsum("bgrpn,bgn->bgrp", updated, read_groups, precision=lax.Precision.HIGHEST)
    head_out = head_out + skip_gain.reshape(group_count, per_group)[None, :, :, None] * input_heads
    head_short = lax.optimization_barrier(head_out.astype(jnp.bfloat16))
    gated = head_short.astype(jnp.float32).reshape(seq_rows, group_count, per_group * HEAD_DIM)
    gated = gated * jax.nn.silu(
        gate_z.astype(jnp.float32).reshape(seq_rows, group_count, per_group * HEAD_DIM)
    )
    gated = (
        gated
        * inverse_rms(gated)
        * group_gain.astype(jnp.float32).reshape(group_count, per_group * HEAD_DIM)[None]
    )
    gated = gated.reshape(seq_rows, head_count * HEAD_DIM).astype(jnp.bfloat16)
    partial_out = jnp.dot(gated, proj_output, preferred_element_type=jnp.float32).astype(
        jnp.bfloat16
    )
    partial_out = lax.optimization_barrier(partial_out).astype(jnp.float32)
    mixed = lax.psum_scatter(
        partial_out.astype(jnp.bfloat16), "tp", scatter_dimension=1, tiled=True
    ).astype(jnp.float32)
    mixed_rows = (residual.astype(jnp.float32) + mixed).astype(jnp.bfloat16)
    return (mixed_rows, updated.reshape(seq_rows, head_count, HEAD_DIM, STATE))


def per_device(
    residual,
    first_gain,
    first_gate,
    first_lift,
    first_down,
    mixer_gain,
    proj_gate,
    proj_input,
    proj_write,
    proj_read,
    proj_step,
    step_bias,
    rate_log,
    skip_gain,
    taps_input,
    taps_write,
    taps_read,
    buffer_input,
    buffer_write,
    buffer_read,
    scan_state,
    group_gain,
    proj_output,
    second_gain,
    second_gate,
    second_lift,
    second_down,
):
    first = half_step(residual, first_gain, first_gate, first_lift, first_down)
    mixed, state_out = state_mixer(
        first,
        mixer_gain,
        proj_gate,
        proj_input,
        proj_write,
        proj_read,
        proj_step,
        step_bias,
        rate_log,
        skip_gain,
        taps_input,
        taps_write,
        taps_read,
        buffer_input,
        buffer_write,
        buffer_read,
        scan_state,
        group_gain,
        proj_output,
    )
    residual_out = half_step(mixed, second_gain, second_gate, second_lift, second_down)
    return (residual_out, state_out)


def solution(mesh):
    placed = (
        P("kv", "tp"),
        P("tp"),
        P("tp", "kv"),
        P("tp", "kv"),
        P("kv", "tp"),
        P(),
        P(None, "tp"),
        P(None, "tp"),
        P(None, "tp"),
        P(None, "tp"),
        P(None, "tp"),
        P("tp"),
        P("tp"),
        P("tp"),
        P(None, "tp"),
        P(None, "tp"),
        P(None, "tp"),
        P("kv", None, "tp"),
        P("kv", None, "tp"),
        P("kv", None, "tp"),
        P("kv", "tp", None, None),
        P("tp"),
        P("tp", None),
        P("tp"),
        P("tp", "kv"),
        P("tp", "kv"),
        P("kv", "tp"),
    )
    return jax.shard_map(
        per_device,
        mesh=mesh,
        in_specs=placed,
        out_specs=(P("kv", "tp"), P("kv", "tp", None, None)),
        check_vma=False,
    )
```

profile of v0, /device:TPU:0, one launch (start us, length us, event | category | flops | bytes accessed | tf_op | source)
XLA Modules:
  0.0 352.4 jit_solution(14504042245031635717)
XLA Ops:
  8.4 8.4 %psum.14 = f32[32]{0:T(128)S(1)} all-reduce(f32[32]{0:T(128)S(1)} %fusion.27), channel_id=1, replica_groups=mesh['kv'=8,'tp'=4] {'tp'}, use_global_device_ids=true, to_apply=%region_1.0 | all-reduce | flops 32 | bytes 256 | tf_op jit(solution)/shard_map/psum | solution.py:18
  18.3 31.2 %all_gather.15 = bf16[256,512]{1,0:T(8,128)(2,1)S(1)} all-gather(bf16[32,512]{1,0:T(8,128)(2,1)S(1)} %fusion.29), channel_id=1, replica_groups=mesh['kv'=8,'tp'=4] {'kv'}, dimensions={0}, use_global_device_ids=true | all-gather | bytes 294912 | tf_op jit(solution)/shard_map/all_gather | solution.py:22
  49.5 1.5 convolution_convert_fusion.3
  51.0 1.5 convolution_convert_fusion.4
  53.8 22.8 %reduce-scatter.16.cloned.1.call-done = bf16[64,1408]{1,0:T(8,128)(2,1)} async-done(((bf16[256,1408]{1,0:T(8,128)(2,1)}), bf16[64,1408]{1,0:T(8,128)(2,1)}) %reduce-scatter.16.cloned.1.call-update) | async-done | bytes 180240 | tf_op jit(solution)/shard_map/reduce_scatter | solution.py:31
  77.6 6.1 %all_gather.16 = bf16[256,704]{1,0:T(8,128)(2,1)S(1)} all-gather(bf16[64,704]{1,0:T(8,128)(2,1)S(1)} %fusion.23), channel_id=1, replica_groups=mesh['kv'=8,'tp'=4] {'tp'}, dimensions={0}, use_global_device_ids=true | all-gather | bytes 450560 | tf_op jit(solution)/shard_map/all_gather | solution.py:35
  83.8 2.2 convolution_convert_fusion.6
  86.4 62.7 %reduce-scatter.10.cloned.1.call-done = bf16[32,512]{1,0:T(8,128)(2,1)} async-done(((bf16[256,512]{1,0:T(8,128)(2,1)}), bf16[32,512]{1,0:T(8,128)(2,1)}) %reduce-scatter.10.cloned.1.call-update) | async-done | bytes 32784 | tf_op jit(solution)/shard_map/reduce_scatter | solution.py:36
  149.9 5.4 %all_gather.17 = bf16[32,2048]{1,0:T(8,128)(2,1)S(1)} all-gather(bf16[32,512]{1,0:T(8,128)(2,1)S(1)} %fusion.30), channel_id=1, replica_groups=mesh['kv'=8,'tp'=4] {'tp'}, dimensions={1}, use_global_device_ids=true | all-gather | bytes 163840 | tf_op jit(solution)/shard_map/all_gather | solution.py:74
  155.4 1.6 divide_multiply_fusion.3
  157.0 1.6 divide_multiply_fusion.2
  158.6 2.1 fusion.7
  161.2 2.1 divide_multiply_fusion.1
  163.6 22.0 %fusion = f32[32,2,1,4,64]{4,2,3,1,0:T(1,128)S(1)} fusion(f32[32,2,128,1,1]{2,3,4,1,0:T(1,128)S(1)} %bitcast.38, f32[32,2,4,64,128]{4,3,2,1,0:T(8,128)} %bitcast.33, f32[32,2,128]{2,1,0:T(2,128)S(1)} %mul.292, f32[32,2,4,64]{3,2,1,0:T(4,128)S(1)} %broadcast_multiply_fusion.1, f32[32,2,4]{2,1,0:T(2,128)S(1)} %copy.40), kind=kOutput, calls=%fused_computation.1 | convolution fusion | flops 31457280 | bytes 8586240 | tf_op jit(solution)/shard_map/bgrpn,bgn->bgrp/dot_general | solution.py:106
  187.6 18.7 %reduce-scatter.12.cloned.1.call-done = bf16[32,512]{1,0:T(8,128)(2,1)} async-done(((bf16[32,2048]{1,0:T(8,128)(2,1)}), bf16[32,512]{1,0:T(8,128)(2,1)}) %reduce-scatter.12.cloned.1.call-update) | async-done | bytes 32784 | tf_op jit(solution)/shard_map/reduce_scatter | solution.py:123
  207.2 5.8 %psum.15 = f32[32]{0:T(128)S(1)} all-reduce(f32[32]{0:T(128)S(1)} %fusion.31), channel_id=1, replica_groups=mesh['kv'=8,'tp'=4] {'tp'}, use_global_device_ids=true, to_apply=%region_11.12 | all-reduce | flops 32 | bytes 256 | tf_op jit(solution)/shard_map/psum | solution.py:18
  213.8 31.4 %all_gather.18 = bf16[256,512]{1,0:T(8,128)(2,1)S(1)} all-gather(bf16[32,512]{1,0:T(8,128)(2,1)S(1)} %fusion.33), channel_id=1, replica_groups=mesh['kv'=8,'tp'=4] {'kv'}, dimensions={0}, use_global_device_ids=true | all-gather | bytes 294912 | tf_op jit(solution)/shard_map/all_gather | solution.py:22
  245.1 1.5 convolution_convert_fusion.1
  246.6 1.5 convolution_convert_fusion.2
  249.7 22.4 %reduce-scatter.18.cloned.1.call-done = bf16[64,1408]{1,0:T(8,128)(2,1)} async-done(((bf16[256,1408]{1,0:T(8,128)(2,1)}), bf16[64,1408]{1,0:T(8,128)(2,1)}) %reduce-scatter.18.cloned.1.call-update) | async-done | bytes 180240 | tf_op jit(solution)/shard_map/reduce_scatter | solution.py:31
  273.2 6.1 %all_gather.19 = bf16[256,704]{1,0:T(8,128)(2,1)S(1)} all-gather(bf16[64,704]{1,0:T(8,128)(2,1)S(1)} %fusion.22), channel_id=1, replica_groups=mesh['kv'=8,'tp'=4] {'tp'}, dimensions={0}, use_global_device_ids=true | all-gather | bytes 450560 | tf_op jit(solution)/shard_map/all_gather | solution.py:35
  279.4 2.2 convolution_convert_fusion.5
  281.6 8.5 %multiply_add_fusion = f32[32,8,64,128]{3,2,1,0:T(8,128)} fusion(f32[32,8,64,128]{3,2,1,0:T(8,128)} %param.47, f32[32,8,128]{2,1,0:T(8,128)S(1)} %bitcast.34, f32[32,8,64]{2,1,0:T(8,128)S(1)} %broadcast_multiply_fusion, f32[32,8]{1,0:T(8,128)S(1)} %copy.43), kind=kLoop, calls=%fused_computation | loop fusion | flops 6291456 | bytes 16974848 | tf_op jit(solution)/shard_map/add | solution.py:103
  290.1 54.4 %reduce-scatter.14.cloned.1.call-done = bf16[32,512]{1,0:T(8,128)(2,1)} async-done(((bf16[256,512]{1,0:T(8,128)(2,1)}), bf16[32,512]{1,0:T(8,128)(2,1)}) %reduce-scatter.14.cloned.1.call-update) | async-done | bytes 32784 | tf_op jit(solution)/shard_map/reduce_scatter | solution.py:36
  (95 shorter events, 14.5 us)
Async XLA Ops:
  7.2 179.2 %copy-start = (bf16[512,2048]{1,0:T(8,128)(2,1)S(1)}, bf16[512,2048]{1,0:T(8,128)(2,1)}, u32[]{:S(2)}) copy-start(bf16[512,2048]{1,0:T(8,128)(2,1)} %param.49) | copy-start | bytes 6291460
  7.2 141.9 %copy-start.1 = (bf16[32,512]{1,0:T(8,128)(2,1)S(1)}, bf16[32,512]{1,0:T(8,128)(2,1)}, u32[]{:S(2)}) copy-start(bf16[32,512]{1,0:T(8,128)(2,1)} %param.27) | copy-start | bytes 98308
  7.2 78.8 %copy-start.7 = (bf16[4,256]{1,0:T(4,128)(2,1)S(1)}, bf16[4,256]{1,0:T(4,128)(2,1)}, u32[]{:S(2)}) copy-start(bf16[4,256]{1,0:T(4,128)(2,1)} %param.42) | copy-start | bytes 6148
  7.2 78.9 %copy-start.8 = (bf16[4,256]{1,0:T(4,128)(2,1)S(1)}, bf16[4,256]{1,0:T(4,128)(2,1)}, u32[]{:S(2)}) copy-start(bf16[4,256]{1,0:T(4,128)(2,1)} %param.43) | copy-start | bytes 6148
  7.2 78.9 %copy-start.6 = (bf16[4,512]{1,0:T(4,128)(2,1)S(1)}, bf16[4,512]{1,0:T(4,128)(2,1)}, u32[]{:S(2)}) copy-start(bf16[4,512]{1,0:T(4,128)(2,1)} %param.41) | copy-start | bytes 12292
  7.2 78.9 %copy-start.13 = (f32[8]{0:T(128)S(1)}, f32[8]{0:T(128)}, u32[]{:S(2)}) copy-start(f32[8]{0:T(128)} %param.39) | copy-start | bytes 100
  7.2 78.9 %copy-start.14 = (f32[8]{0:T(128)S(1)}, f32[8]{0:T(128)}, u32[]{:S(2)}) copy-start(f32[8]{0:T(128)} %param.40) | copy-start | bytes 100
  7.2 79.0 %copy-start.10 = (bf16[512]{0:T(512)(128)(2,1)S(1)}, bf16[512]{0:T(512)(128)(2,1)}, u32[]{:S(2)}) copy-start(bf16[512]{0:T(512)(128)(2,1)} %param.48) | copy-start | bytes 3076
  7.3 79.0 %copy-start.9 = (bf16[2048]{0:T(1024)(128)(2,1)S(1)}, bf16[2048]{0:T(1024)(128)(2,1)}, u32[]{:S(2)}) copy-start(bf16[2048]{0:T(1024)(128)(2,1)} %param.32) | copy-start | bytes 12292
  7.3 79.0 %copy-start.4 = (bf16[32,3,256]{2,0,1:T(8,128)(2,1)S(1)}, bf16[32,3,256]{2,0,1:T(8,128)(2,1)}, u32[]{:S(2)}) copy-start(bf16[32,3,256]{2,0,1:T(8,128)(2,1)} %param.46) | copy-start | bytes 147460
  7.3 79.0 %copy-start.5 = (bf16[32,3,256]{2,0,1:T(8,128)(2,1)S(1)}, bf16[32,3,256]{2,0,1:T(8,128)(2,1)}, u32[]{:S(2)}) copy-start(bf16[32,3,256]{2,0,1:T(8,128)(2,1)} %param.45) | copy-start | bytes 147460
  7.3 79.1 %copy-start.3 = (bf16[32,3,512]{2,0,1:T(8,128)(2,1)S(1)}, bf16[32,3,512]{2,0,1:T(8,128)(2,1)}, u32[]{:S(2)}) copy-start(bf16[32,3,512]{2,0,1:T(8,128)(2,1)} %param.44) | copy-start | bytes 294916
  7.3 153.4 %copy-start.15 = (f32[8]{0:T(128)S(1)}, f32[8]{0:T(128)}, u32[]{:S(2)}) copy-start(f32[8]{0:T(128)} %param.38) | copy-start | bytes 100
  7.3 153.4 %copy-start.12 = (bf16[2048,8]{0,1:T(8,128)(2,1)S(1)}, bf16[2048,8]{0,1:T(8,128)(2,1)}, u32[]{:S(2)}) copy-start(bf16[2048,8]{0,1:T(8,128)(2,1)} %param.37) | copy-start | bytes 98308
  7.3 69.3 %reduce-scatter.16.cloned.1.call-start = ((), (), s32[]{:S(2)}) async-start(), calls=%async_computation.8 | async-start | bytes 901120 | tf_op jit(solution)/shard_map/reduce_scatter | solution.py:31
  53.8 95.3 %reduce-scatter.10.cloned.1.call-start = ((), (), s32[]{:S(2)}) async-start(), calls=%async_computation.5 | async-start | bytes 294912 | tf_op jit(solution)/shard_map/reduce_scatter | solution.py:36
  86.0 120.3 %reduce-scatter.12.cloned.1.call-start = ((), (), s32[]{:S(2)}) async-start(), calls=%async_computation.6 | async-start | bytes 163840 | tf_op jit(solution)/shard_map/reduce_scatter | solution.py:123
  160.8 26.8 %copy-start.11 = (bf16[512]{0:T(512)(128)(2,1)S(1)}, bf16[512]{0:T(512)(128)(2,1)}, u32[]{:S(2)}) copy-start(bf16[512]{0:T(512)(128)(2,1)} %param.50) | copy-start | bytes 3076
  187.5 84.7 %reduce-scatter.18.cloned.1.call-start = ((), (), s32[]{:S(2)}) async-start(), calls=%async_computation.9 | async-start | bytes 901120 | tf_op jit(solution)/shard_map/reduce_scatter | solution.py:31
  249.4 95.1 %reduce-scatter.14.cloned.1.call-start = ((), (), s32[]{:S(2)}) async-start(), calls=%async_computation.7 | async-start | bytes 294912 | tf_op jit(solution)/shard_map/reduce_scatter | solution.py:36
  281.6 62.9 %copy-start.2 = (bf16[32,512]{1,0:T(8,128)(2,1)S(1)}, bf16[32,512]{1,0:T(8,128)(2,1)}, u32[]{:S(2)}) copy-start(bf16[32,512]{1,0:T(8,128)(2,1)} %reduce-scatter.12.cloned.1.call-done) | copy-start | bytes 98308
Sparse Core Ops, SparseCore 0:
  53.9 22.6 reduce-scatter.15
  86.1 62.9 reduce-scatter.9
  187.6 18.6 reduce-scatter.11
  249.5 22.6 reduce-scatter.17
  281.7 62.7 reduce-scatter.13
where the time goes:
time: 353 us; the launch traced here: 352 us
  waiting for transfers between devices  181 us (51%)
  blocking collectives  94.4 us (27%)
  matrix products  41.1 us (12%)
  other arithmetic  18 us (5%)
  between operations  14.3 us (4%)
    reduce_scatter x2, waiting for transfers between devices, half_step(): lax.psum_scatter(jnp.dot(hidden, down_weight, preferred_element_type=jnp....  117 us
    all_gather x2, blocking collectives, half_step(): row_piece = lax.all_gather(normed, 'kv', axis=0, tiled=True)  62.6 us
    reduce_scatter x2, waiting for transfers between devices, half_step(): lax.psum_scatter(partial_value.astype(jnp.bfloat16), 'tp', scatter_dimens...  45.2 us
    dot_general x1, matrix products, state_mixer(): jnp.einsum('bgrpn,bgn->bgrp', updated, read_groups, precision=lax.Precisi...  22 us
    reduce_scatter x1, waiting for transfers between devices, state_mixer(): lax.psum_scatter(partial_out.astype(jnp.bfloat16), 'tp', scatter_dimensio...  18.7 us
    psum x2, blocking collectives, half_step(): row_total = lax.psum(jnp.sum(widened * widened, axis=1), 'tp')  14.1 us
    all_gather x2, blocking collectives, half_step(): hidden = lax.all_gather(active, 'tp', axis=0, tiled=True)  12.3 us
    add x1, other arithmetic, state_mixer(): retain_g[..., None, None] * old_state  8.5 us
  transfers between devices with their start and end apart: 5, of which 5 were waited for; matrix products, arithmetic and copies ran while one was open for 3% of the time, Pallas kernels for 0%

commit v1 on v0

--- a/solution.py
+++ b/solution.py
@@ -2,11 +2,15 @@
 import jax.numpy as jnp
 from jax import lax
 from jax.sharding import PartitionSpec as P
+from jax.lax import all_to_all, psum
 
 D = 2048
 HEAD_DIM = 64
 STATE = 128
 norm_eps = 1e-06
+see_the_edge = lambda arr_in: jnp.concatenate(
+    all_to_all(jnp.stack([arr_in] * psum(1, "kv")), "kv", 0, 0), axis=0
+)
 
 
 def inverse_rms(values):
@@ -19,7 +23,7 @@
     factor = lax.rsqrt(row_total / D + norm_eps)
     normed = (widened * factor[:, None] * gain.astype(jnp.float32)[None, :]).astype(jnp.bfloat16)
     hidden_cols = gate_weight.shape[1]
-    row_piece = lax.all_gather(normed, "kv", axis=0, tiled=True)
+    row_piece = see_the_edge(normed)
     gate_part = jnp.dot(row_piece, gate_weight, preferred_element_type=jnp.float32).astype(
         jnp.bfloat16
     )

time: 353 us -> 315 us (0.89)
  blocking collectives: 94.4 us -> 59.9 us
  waiting for transfers between devices: 181 us -> 174 us
    all_gather x2 -> x0, blocking collectives: 62.6 us -> none  [half_step(): row_piece = lax.all_gather(normed, 'kv', axis=0, tiled=True)]
    all_to_all x0 -> x2, blocking collectives: none -> 28 us  [all_to_all(jnp.stack([arr_in] * psum(1, 'kv')), 'kv', 0, 0)]
    reduce_scatter x2, waiting for transfers between devices: 117 us -> 113 us  [half_step(): lax.psum_scatter(jnp.dot(hidden, down_weight, preferred_element_type=jnp....]
  transfers between devices with their start and end apart: 5 -> 5, of which waited for: 5 -> 5; matrix products, arithmetic and copies ran while one was open for 3% -> 4% of each run, Pallas kernels for 0% -> 0%
where the time goes in v1:
time: 315 us; the launch traced here: 314 us
  waiting for transfers between devices  174 us (55%)
  blocking collectives  59.9 us (19%)
  matrix products  39.9 us (13%)
  other arithmetic  21.2 us (7%)
  between operations  14.1 us (4%)
  local copies, waits for them, and re-layouts  4.73 us (2%)
    reduce_scatter x2, waiting for transfers between devices, half_step(): lax.psum_scatter(jnp.dot(hidden, down_weight, preferred_element_type=jnp....  113 us
    reduce_scatter x2, waiting for transfers between devices, half_step(): lax.psum_scatter(partial_value.astype(jnp.bfloat16), 'tp', scatter_dimens...  42.1 us
    all_to_all x2, blocking collectives, all_to_all(jnp.stack([arr_in] * psum(1, 'kv')), 'kv', 0, 0)  28 us
    dot_general x1, matrix products, state_mixer(): jnp.einsum('bgrpn,bgn->bgrp', updated, read_groups, precision=lax.Precisi...  22 us
    reduce_scatter x1, waiting for transfers between devices, state_mixer(): lax.psum_scatter(partial_out.astype(jnp.bfloat16), 'tp', scatter_dimensio...  18.7 us
    psum x2, blocking collectives, half_step(): row_total = lax.psum(jnp.sum(widened * widened, axis=1), 'tp')  14.1 us
    all_gather x2, blocking collectives, half_step(): hidden = lax.all_gather(active, 'tp', axis=0, tiled=True)  12.3 us
    add x1, other arithmetic, state_mixer(): retain_g[..., None, None] * old_state  8.5 us
  transfers between devices with their start and end apart: 5, of which 5 were waited for; matrix products, arithmetic and copies ran while one was open for 4% of the time, Pallas kernels for 0%

profile of v1, /device:TPU:0, one launch (start us, length us, event | category | flops | bytes accessed | tf_op | source)
XLA Modules:
  0.0 313.6 jit_solution(5556013366093624469)
XLA Ops:
  8.3 8.4 %psum.14 = f32[32]{0:T(128)S(1)} all-reduce(f32[32]{0:T(128)S(1)} %fusion.27), channel_id=1, replica_groups=mesh['kv'=8,'tp'=4] {'tp'}, use_global_device_ids=true, to_apply=%region_1.0 | all-reduce | flops 32 | bytes 256 | tf_op jit(solution)/shard_map/psum | solution.py:22
  18.2 13.9 %all_to_all.10 = bf16[8,32,512]{2,1,0:T(8,128)(2,1)S(1)} all-to-all(bf16[8,32,512]{2,1,0:T(8,128)(2,1)S(1)} %stack.4), channel_id=1, replica_groups=mesh['kv'=8,'tp'=4] {'kv'}, dimensions={0} | all-to-all | bytes 524288 | tf_op jit(solution)/shard_map/all_to_all | solution.py:12
  32.1 1.5 convolution_convert_fusion.3
  33.6 1.5 convolution_convert_fusion.4
  36.3 21.4 %reduce-scatter.16.cloned.1.call-done = bf16[64,1408]{1,0:T(8,128)(2,1)} async-done(((bf16[256,1408]{1,0:T(8,128)(2,1)}), bf16[64,1408]{1,0:T(8,128)(2,1)}) %reduce-scatter.16.cloned.1.call-update) | async-done | bytes 180240 | tf_op jit(solution)/shard_map/reduce_scatter | solution.py:35
  58.9 6.1 %all_gather.9 = bf16[256,704]{1,0:T(8,128)(2,1)S(1)} all-gather(bf16[64,704]{1,0:T(8,128)(2,1)S(1)} %fusion.23), channel_id=1, replica_groups=mesh['kv'=8,'tp'=4] {'tp'}, dimensions={0}, use_global_device_ids=true | all-gather | bytes 450560 | tf_op jit(solution)/shard_map/all_gather | solution.py:39
  70.9 58.4 %reduce-scatter.10.cloned.1.call-done = bf16[32,512]{1,0:T(8,128)(2,1)} async-done(((bf16[256,512]{1,0:T(8,128)(2,1)}), bf16[32,512]{1,0:T(8,128)(2,1)}) %reduce-scatter.10.cloned.1.call-update) | async-done | bytes 32784 | tf_op jit(solution)/shard_map/reduce_scatter | solution.py:40
  130.1 5.4 %all_gather.10 = bf16[32,2048]{1,0:T(8,128)(2,1)S(1)} all-gather(bf16[32,512]{1,0:T(8,128)(2,1)S(1)} %fusion.30), channel_id=1, replica_groups=mesh['kv'=8,'tp'=4] {'tp'}, dimensions={1}, use_global_device_ids=true | all-gather | bytes 163840 | tf_op jit(solution)/shard_map/all_gather | solution.py:78
  135.6 1.6 divide_multiply_fusion.3
  137.2 1.6 divide_multiply_fusion.2
  138.8 2.1 fusion.7
  141.4 2.1 divide_multiply_fusion.1
  143.8 22.0 %fusion = f32[32,2,1,4,64]{4,2,3,1,0:T(1,128)S(1)} fusion(f32[32,2,128,1,1]{2,3,4,1,0:T(1,128)S(1)} %bitcast.44, f32[32,2,4,64,128]{4,3,2,1,0:T(8,128)} %bitcast.35, f32[32,2,128]{2,1,0:T(2,128)S(1)} %mul.292, f32[32,2,4,64]{3,2,1,0:T(4,128)S(1)} %broadcast_multiply_fusion.1, f32[32,2,4]{2,1,0:T(2,128)S(1)} %copy.40), kind=kOutput, calls=%fused_computation.1 | convolution fusion | flops 31457280 | bytes 8586240 | tf_op jit(solution)/shard_map/bgrpn,bgn->bgrp/dot_general | solution.py:110
  167.8 18.7 %reduce-scatter.12.cloned.1.call-done = bf16[32,512]{1,0:T(8,128)(2,1)} async-done(((bf16[32,2048]{1,0:T(8,128)(2,1)}), bf16[32,512]{1,0:T(8,128)(2,1)}) %reduce-scatter.12.cloned.1.call-update) | async-done | bytes 32784 | tf_op jit(solution)/shard_map/reduce_scatter | solution.py:127
  187.4 5.8 %psum.15 = f32[32]{0:T(128)S(1)} all-reduce(f32[32]{0:T(128)S(1)} %fusion.31), channel_id=1, replica_groups=mesh['kv'=8,'tp'=4] {'tp'}, use_global_device_ids=true, to_apply=%region_11.12 | all-reduce | flops 32 | bytes 256 | tf_op jit(solution)/shard_map/psum | solution.py:22
  194.0 14.2 %all_to_all.11 = bf16[8,32,512]{2,1,0:T(8,128)(2,1)S(1)} all-to-all(bf16[8,32,512]{2,1,0:T(8,128)(2,1)S(1)} %stack.5), channel_id=1, replica_groups=mesh['kv'=8,'tp'=4] {'kv'}, dimensions={0} | all-to-all | bytes 524288 | tf_op jit(solution)/shard_map/all_to_all | solution.py:12
  208.2 1.5 convolution_convert_fusion.1
  209.7 1.5 convolution_convert_fusion.2
  212.8 20.6 %reduce-scatter.18.cloned.1.call-done = bf16[64,1408]{1,0:T(8,128)(2,1)} async-done(((bf16[256,1408]{1,0:T(8,128)(2,1)}), bf16[64,1408]{1,0:T(8,128)(2,1)}) %reduce-scatter.18.cloned.1.call-update) | async-done | bytes 180240 | tf_op jit(solution)/shard_map/reduce_scatter | solution.py:35
  234.5 6.1 %all_gather.11 = bf16[256,704]{1,0:T(8,128)(2,1)S(1)} all-gather(bf16[64,704]{1,0:T(8,128)(2,1)S(1)} %fusion.22), channel_id=1, replica_groups=mesh['kv'=8,'tp'=4] {'tp'}, dimensions={0}, use_global_device_ids=true | all-gather | bytes 450560 | tf_op jit(solution)/shard_map/all_gather | solution.py:39
  240.6 2.2 convolution_convert_fusion.5
  242.9 8.5 %multiply_add_fusion = f32[32,8,64,128]{3,2,1,0:T(8,128)} fusion(f32[32,8,64,128]{3,2,1,0:T(8,128)} %param.47, f32[32,8,128]{2,1,0:T(8,128)S(1)} %bitcast.40, f32[32,8,64]{2,1,0:T(8,128)S(1)} %broadcast_multiply_fusion, f32[32,8]{1,0:T(8,128)S(1)} %copy.43), kind=kLoop, calls=%fused_computation | loop fusion | flops 6291456 | bytes 16974848 | tf_op jit(solution)/shard_map/add | solution.py:107
  251.4 54.4 %reduce-scatter.14.cloned.1.call-done = bf16[32,512]{1,0:T(8,128)(2,1)} async-done(((bf16[256,512]{1,0:T(8,128)(2,1)}), bf16[32,512]{1,0:T(8,128)(2,1)}) %reduce-scatter.14.cloned.1.call-update) | async-done | bytes 32784 | tf_op jit(solution)/shard_map/reduce_scatter | solution.py:40
  305.7 1.4 fusion.34
  (85 shorter events, 18.7 us)
Async XLA Ops:
  7.2 159.4 %copy-start = (bf16[512,2048]{1,0:T(8,128)(2,1)S(1)}, bf16[512,2048]{1,0:T(8,128)(2,1)}, u32[]{:S(2)}) copy-start(bf16[512,2048]{1,0:T(8,128)(2,1)} %param.49) | copy-start | bytes 6291460
  7.2 57.8 %copy-start.1 = (bf16[704,512]{1,0:T(8,128)(2,1)S(1)}, bf16[704,512]{1,0:T(8,128)(2,1)}, u32[]{:S(2)}) copy-start(bf16[704,512]{1,0:T(8,128)(2,1)} %param.31) | copy-start | bytes 2162692
  7.2 59.0 %copy-start.4 = (bf16[4,256]{1,0:T(4,128)(2,1)S(1)}, bf16[4,256]{1,0:T(4,128)(2,1)}, u32[]{:S(2)}) copy-start(bf16[4,256]{1,0:T(4,128)(2,1)} %param.42) | copy-start | bytes 6148
  7.2 59.0 %copy-start.5 = (bf16[4,256]{1,0:T(4,128)(2,1)S(1)}, bf16[4,256]{1,0:T(4,128)(2,1)}, u32[]{:S(2)}) copy-start(bf16[4,256]{1,0:T(4,128)(2,1)} %param.43) | copy-start | bytes 6148
  7.2 59.0 %copy-start.3 = (bf16[4,512]{1,0:T(4,128)(2,1)S(1)}, bf16[4,512]{1,0:T(4,128)(2,1)}, u32[]{:S(2)}) copy-start(bf16[4,512]{1,0:T(4,128)(2,1)} %param.41) | copy-start | bytes 12292
  7.2 61.1 %copy-start.6 = (bf16[2048]{0:T(1024)(128)(2,1)S(1)}, bf16[2048]{0:T(1024)(128)(2,1)}, u32[]{:S(2)}) copy-start(bf16[2048]{0:T(1024)(128)(2,1)} %param.32) | copy-start | bytes 12292
  7.2 50.6 %reduce-scatter.16.cloned.1.call-start = ((), (), s32[]{:S(2)}) async-start(), calls=%async_computation.10 | async-start | bytes 901120 | tf_op jit(solution)/shard_map/reduce_scatter | solution.py:35
  36.3 104.7 %copy-start.8 = (bf16[2048,8]{0,1:T(8,128)(2,1)S(1)}, bf16[2048,8]{0,1:T(8,128)(2,1)}, u32[]{:S(2)}) copy-start(bf16[2048,8]{0,1:T(8,128)(2,1)} %param.37) | copy-start | bytes 98308
  36.3 104.7 %copy-start.9 = (f32[8]{0:T(128)S(1)}, f32[8]{0:T(128)}, u32[]{:S(2)}) copy-start(f32[8]{0:T(128)} %param.38) | copy-start | bytes 100
  36.3 93.0 %reduce-scatter.10.cloned.1.call-start = ((), (), s32[]{:S(2)}) async-start(), calls=%async_computation.7 | async-start | bytes 294912 | tf_op jit(solution)/shard_map/reduce_scatter | solution.py:40
  66.1 120.4 %reduce-scatter.12.cloned.1.call-start = ((), (), s32[]{:S(2)}) async-start(), calls=%async_computation.8 | async-start | bytes 163840 | tf_op jit(solution)/shard_map/reduce_scatter | solution.py:127
  140.9 26.8 %copy-start.7 = (bf16[512]{0:T(512)(128)(2,1)S(1)}, bf16[512]{0:T(512)(128)(2,1)}, u32[]{:S(2)}) copy-start(bf16[512]{0:T(512)(128)(2,1)} %param.50) | copy-start | bytes 3076
  167.7 65.7 %reduce-scatter.18.cloned.1.call-start = ((), (), s32[]{:S(2)}) async-start(), calls=%async_computation.11 | async-start | bytes 901120 | tf_op jit(solution)/shard_map/reduce_scatter | solution.py:35
  212.4 93.3 %reduce-scatter.14.cloned.1.call-start = ((), (), s32[]{:S(2)}) async-start(), calls=%async_computation.9 | async-start | bytes 294912 | tf_op jit(solution)/shard_map/reduce_scatter | solution.py:40
  242.9 62.9 %copy-start.2 = (bf16[32,512]{1,0:T(8,128)(2,1)S(1)}, bf16[32,512]{1,0:T(8,128)(2,1)}, u32[]{:S(2)}) copy-start(bf16[32,512]{1,0:T(8,128)(2,1)} %reduce-scatter.12.cloned.1.call-done) | copy-start | bytes 98308
Sparse Core Ops, SparseCore 0:
  36.4 21.3 reduce-scatter.15
  66.2 62.9 reduce-scatter.9
  167.8 18.6 reduce-scatter.11
  212.5 20.8 reduce-scatter.17
  242.9 62.7 reduce-scatter.13
